TPU v7x, 1024 devices: a whole 4x4x32 slice. The times are simulated.
1024 devices in a mesh: fs: 64 (over z, core), tp: 16 (over y, x).
Axes of the slice: x: 4, y: 4, z: 32, core: 2. Of those that a mesh axis runs over, the one named last changes fastest.
Arguments:
- prompt: bfloat16 [4096, 2048], P('tp'), may hold values from -6 to 6
- norm_gain: float32 [2048], P('fs'), may hold values from 0.1 to 1.9
- gate_master: float32 [32, 2048, 512], P(None, 'fs', 'tp'), may hold values from -6 to 6
- up_master: float32 [32, 2048, 512], P(None, 'fs', 'tp'), may hold values from -6 to 6
- down_master: float32 [32, 2048, 512], P(None, 'fs', 'tp'), may hold values from -6 to 6
- group_choice: int32 [4096], P('tp'), may hold values from 0 to 3
- inner_choice: int32 [4096, 2], P('tp'), may hold values from 0 to 7, as said below
- route_weight: float32 [4096, 2], P('tp'), may hold values from 0.2 to 1
Outputs:
- gate_served: bfloat16 [2048, 16384], P(None, 'fs')
- up_served: bfloat16 [2048, 16384], P(None, 'fs')
- down_served: bfloat16 [2048, 16384], P(None, 'fs')
- mixed: bfloat16 [4096, 2048], P('tp', 'fs')
Inputs may be any that keep to these rules, and one draw needn't show every extreme that they name: `inner_choice`: the two experts of a token differ.
All inputs are finite; a program needn't handle non-finite values.
Results may differ from a plain program's by a relative error of at most 0.0081.
Values may be sent and summed in bfloat16 or wider, within the bound.
A program may use at most 64 MiB of HBM per device.

v0:
```python
import jax
import jax.numpy as jnp
from jax import lax
from jax.sharding import Mesh
from jax.sharding import PartitionSpec as P

FF = 512
GROUPS = 4
EPG = 8
FS = ("fs_0", "fs_1")


def in_blocks(value, dim, devices):
    shape = value.shape
    parts = value.reshape(*shape[:dim], devices, shape[dim] // devices, *shape[dim + 1 :])
    return jnp.moveaxis(parts, dim, 0)


def laid_out(parts, dim):
    parts = jnp.moveaxis(parts, 0, dim)
    shape = parts.shape
    return parts.reshape(*shape[:dim], shape[dim] * shape[dim + 1], *shape[dim + 2 :])


def turned_blocks(parts, axes, order):
    inside = parts.shape[1:]
    filled = parts.reshape(*(lax.axis_size(a) for a in axes), *inside)
    for k in order:
        filled = lax.all_to_all(filled, axes[k], k, k, tiled=True)
    return filled.reshape(-1, *inside)


def two_step_exchange(value, groups, order, split_dim, concat_dim):
    devices = lax.axis_size(groups[0]) * lax.axis_size(groups[1])
    parts = in_blocks(value, split_dim, devices)
    return laid_out(turned_blocks(parts, groups, order), concat_dim)


def copy_for_each(value, axis):
    devices = lax.axis_size(axis)
    return lax.all_to_all(
        jnp.broadcast_to(value[None], (devices, *value.shape)), axis, 0, 0, tiled=True
    )


def gathered_copies(value, axis, dim):
    parts = copy_for_each(value, axis)
    return laid_out(parts, dim)


def reduced_to_own(parts, axes, order):
    inside = parts.shape[1:]
    parts = parts.reshape(*(lax.axis_size(a) for a in axes), *inside)
    parts = jnp.moveaxis(parts, order, range(len(axes))).reshape(-1, *inside)
    for k in order:
        parts = lax.psum_scatter(parts, axes[k], scatter_dimension=0, tiled=True)
    return parts[0]


def scatter_axes(value, axes, order, dim):
    devices = lax.axis_size(axes)
    return reduced_to_own(in_blocks(value, dim, devices), axes, order)


def flatten_rows(piece):
    count, experts, rows, hidden = piece.shape
    return piece.transpose(0, 2, 1, 3).reshape(count, rows, experts * hidden)


def restore_rows(gathered, rows):
    parts = lax.axis_size("tp")
    count, total, width = gathered.shape
    blocks = total // (parts * rows)
    ordered = gathered.reshape(count, parts, blocks, rows, width).transpose(0, 2, 1, 3, 4)
    return ordered.reshape(count, total, width)


def activations(normed, gate_local, up_local, column_weight):
    width = normed.shape[1]
    gate_act = jnp.dot(normed, gate_local, preferred_element_type=jnp.float32) * width ** (-0.5)
    up_act = jnp.dot(normed, up_local, preferred_element_type=jnp.float32) * width ** (-0.5)
    return (column_weight * jax.nn.silu(gate_act) * up_act).astype(jnp.bfloat16)


def route_columns(weight, columns, experts):
    first = lax.axis_index(FS) * columns
    owner = (first + jnp.arange(columns, dtype=jnp.int32)) // FF
    onehot = (owner[None, :] == jnp.arange(experts, dtype=jnp.int32)[:, None]).astype(jnp.float32)
    return jnp.dot(weight, onehot, precision=lax.Precision.HIGHEST)


def shards(
    prompt, norm_gain, gate_master, up_master, down_master, group_choice, inner_choice, route_weight
):
    experts = GROUPS * EPG
    scale = norm_gain[None, :, None]
    gate_cast = (gate_master * scale).astype(jnp.bfloat16)
    up_cast = (up_master * scale).astype(jnp.bfloat16)
    down_cast = down_master.astype(jnp.bfloat16)
    rows = gate_master.shape[1] // lax.axis_size("tp")
    values = prompt.astype(jnp.float32)
    normed = (values * lax.rsqrt(jnp.mean(values * values, axis=1, keepdims=True) + 1e-06)).astype(
        jnp.bfloat16
    )
    chosen = group_choice[:, None] * EPG + inner_choice
    member = (chosen[:, :, None] == jnp.arange(experts, dtype=jnp.int32)[None, None, :]).astype(
        jnp.float32
    )
    weight = jnp.sum(member * route_weight[:, :, None], axis=1)
    stacked = jnp.stack([gate_cast, up_cast, down_cast])
    widened = lax.all_to_all(stacked, "tp", split_axis=2, concat_axis=3, tiled=True)
    moved = two_step_exchange(flatten_rows(widened), ("fs_0", "fs_1"), (1, 0), 2, 1)
    served = restore_rows(gathered_copies(moved, "tp", 1), rows)
    gate_local, up_local, down_local = (served[0], served[1], served[2])
    column_weight = route_columns(weight, gate_local.shape[1], experts)
    scaled = activations(normed, gate_local, up_local, column_weight)
    summed = scatter_axes(
        lax.dot_general(
            down_local, scaled, (((1,), (1,)), ((), ())), preferred_element_type=jnp.float32
        ),
        FS,
        (1, 0),
        0,
    )
    mixed = (summed * FF ** (-0.5)).T.astype(jnp.bfloat16)
    return (gate_local, up_local, down_local, mixed)


def solution(mesh):
    split = Mesh(mesh.devices.reshape(32, 2, mesh.shape["tp"]), ("fs_0", "fs_1", "tp"))
    in_specs = (
        P("tp", None),
        P(FS),
        P(None, FS, "tp"),
        P(None, FS, "tp"),
        P(None, FS, "tp"),
        P("tp"),
        P("tp", None),
        P("tp", None),
    )
    out_specs = (P(None, FS), P(None, FS), P(None, FS), P("tp", FS))
    return jax.shard_map(
        shards, mesh=split, in_specs=in_specs, out_specs=out_specs, check_vma=False
    )
```

profile of v0, /device:TPU:4, one launch (start us, length us, event | category | flops | bytes accessed | tf_op | source)
XLA Modules:
  0.0 327.7 jit_solution(2925411045151744883)
XLA Ops:
  7.2 1.4 copy.92
  8.5 1.8 fusion.9
  10.5 0.8 reshape.66
  11.3 21.6 %all_to_all.33 = bf16[16,2,3072]{2,1,0:T(2,128)(2,1)S(1)} all-to-all(bf16[16,2,3072]{2,1,0:T(2,128)(2,1)S(1)} %reshape.66), channel_id=1, replica_groups=mesh['fs_0'=32,'fs_1'=2,'tp'=16] {'tp'}, dimensions={0} | all-to-all | bytes 393216 | tf_op jit(solution)/shard_map/all_to_all | solution.py:111
  33.8 0.7 all_to_all.25
  34.7 3.9 %all_to_all.34 = bf16[32,2,3,2,256]{4,0,3,2,1:T(8,128)(2,1)S(1)} all-to-all(bf16[32,2,3,2,256]{4,0,3,2,1:T(8,128)(2,1)S(1)} %copy.66), channel_id=1, replica_groups=mesh['fs_0'=32,'fs_1'=2,'tp'=16] {'fs_1'}, dimensions={1} | all-to-all | bytes 393216 | tf_op jit(solution)/shard_map/all_to_all | solution.py:29
  38.8 57.5 %all_to_all.35 = bf16[32,2,3,2,256]{4,1,3,2,0:T(2,128)(2,1)S(1)} all-to-all(bf16[32,2,3,2,256]{4,1,3,2,0:T(2,128)(2,1)S(1)} %copy.67), channel_id=1, replica_groups=mesh['fs_0'=32,'fs_1'=2,'tp'=16] {'fs_0'}, dimensions={0} | all-to-all | bytes 393216 | tf_op jit(solution)/shard_map/all_to_all | solution.py:29
  96.7 2.0 broadcast_in_dim.5
  98.7 6.1 %all-to-all-start.3 = ((bf16[16,3,128,256]{3,2,1,0:T(8,128)(2,1)}), bf16[16,3,128,256]{3,2,1,0:T(8,128)(2,1)S(1)}, u32[]{:S(2)}, u32[]{:S(2)}) async-start(bf16[16,3,128,256]{3,2,1,0:T(8,128)(2,1)} %broadcast_in_dim.5), calls=%async_computation.3 | async-start | bytes 6291456 | tf_op jit(solution)/shard_map/all_to_all | solution.py:41
  105.2 1.5 fusion
  106.7 37.1 %all-to-all-done.3 = bf16[16,3,128,256]{3,2,1,0:T(8,128)(2,1)S(1)} async-done(((bf16[16,3,128,256]{3,2,1,0:T(8,128)(2,1)}), bf16[16,3,128,256]{3,2,1,0:T(8,128)(2,1)S(1)}, u32[]{:S(2)}, u32[]{:S(2)}) %all-to-all-start.3) | async-done | bytes 3145760 | tf_op jit(solution)/shard_map/all_to_all | solution.py:41
  143.8 1.8 copy.70
  145.6 1.6 fusion.14
  147.3 1.1 copy.73
  148.8 2.3 copy.72
  151.1 1.2 squeeze.11
  152.3 2.3 copy.71
  154.6 1.2 squeeze.10
  155.8 2.2 convolution_multiply_fusion.1
  159.3 1.5 copy.75
  160.9 17.6 %reduce-scatter.3.cloned.1.call-done = f32[32,32,256]{2,1,0:T(8,128)} async-done(((f32[64,32,256]{2,1,0:T(8,128)}), f32[32,32,256]{2,1,0:T(8,128)}) %reduce-scatter.3.cloned.1.call-update) | async-done | bytes 1048592 | tf_op jit(solution)/shard_map/reduce_scatter | solution.py:56
  178.5 1.2 squeeze.12
  179.7 139.7 %reduce-scatter.5.cloned.1.call-done = f32[1,32,256]{2,1,0:T(8,128)} async-done(((f32[32,32,256]{2,1,0:T(8,128)}), f32[1,32,256]{2,1,0:T(8,128)}) %reduce-scatter.5.cloned.1.call-update) | async-done | bytes 32784 | tf_op jit(solution)/shard_map/reduce_scatter | solution.py:56
  319.5 1.4 fusion.12
  (33 shorter events, 3.9 us)
Async XLA Ops:
  98.7 6.4 %copy-start.4 = (s32[256]{0:T(256)S(1)}, s32[256]{0:T(256)}, u32[]{:S(2)}) copy-start(s32[256]{0:T(256)} %param.13) | copy-start | bytes 3076
  98.7 6.4 %copy-start.3 = (s32[256,2]{0,1:T(2,128)S(1)}, s32[256,2]{0,1:T(2,128)}, u32[]{:S(2)}) copy-start(s32[256,2]{0,1:T(2,128)} %param.14) | copy-start | bytes 6148
  98.7 6.4 %copy-start.2 = (f32[256,2]{0,1:T(2,128)S(1)}, f32[256,2]{0,1:T(2,128)}, u32[]{:S(2)}) copy-start(f32[256,2]{0,1:T(2,128)} %param.15) | copy-start | bytes 6148
  98.7 45.1 %all-to-all-start.3 = ((bf16[16,3,128,256]{3,2,1,0:T(8,128)(2,1)}), bf16[16,3,128,256]{3,2,1,0:T(8,128)(2,1)S(1)}, u32[]{:S(2)}, u32[]{:S(2)}) async-start(bf16[16,3,128,256]{3,2,1,0:T(8,128)(2,1)} %broadcast_in_dim.5), calls=%async_computation.3 | async-start | bytes 6291456 | tf_op jit(solution)/shard_map/all_to_all | solution.py:41
  104.9 73.6 %reduce-scatter.3.cloned.1.call-start = ((), (), s32[]{:S(2)}) async-start(), calls=%async_computation.6 | async-start | bytes 3145728 | tf_op jit(solution)/shard_map/reduce_scatter | solution.py:56
  155.8 2.2 copy-start
  155.8 2.2 copy-start.1
  160.8 158.6 %reduce-scatter.5.cloned.1.call-start = ((), (), s32[]{:S(2)}) async-start(), calls=%async_computation.7 | async-start | bytes 1081344 | tf_op jit(solution)/shard_map/reduce_scatter | solution.py:56
Sparse Core Ops, SparseCore 0:
  161.0 17.4 reduce-scatter.2
  181.9 137.5 reduce-scatter.4
where the time goes:
time: 328 us
  waiting for transfers between devices  194 us (59%)
  blocking collectives  83 us (25%)
  local copies, waits for them, and re-layouts  21.1 us (6%)
  between operations  14.3 us (4%)
  starting transfers between devices  6.39 us (2%)
  other arithmetic  4.93 us (2%)
  matrix products  3.47 us (1%)
    reduce_scatter x2, waiting for transfers between devices, reduced_to_own(): parts = lax.psum_scatter(parts, axes[k], scatter_dimension=0, tiled=True)  157 us
    all_to_all x2, blocking collectives, turned_blocks(): filled = lax.all_to_all(filled, axes[k], k, k, tiled=True)  61.4 us
    all_to_all x1, waiting for transfers between devices, copy_for_each(): lax.all_to_all(jnp.broadcast_to(value[None], (devices, *value.shape)), ax...  37.1 us
    all_to_all x1, blocking collectives, shards(): lax.all_to_all(stacked, 'tp', split_axis=2, concat_axis=3, tiled=True)  21.6 us
    slice x4, local copies, waits for them, and re-layouts, shards(): gate_local, up_local, down_local = (served[0], served[1], served[2])  7.29 us
  transfers between devices with their start and end apart: 3, of which 3 were waited for; matrix products, arithmetic and copies ran while one was open for 1% of the time, Pallas kernels for 0%

commit v1 on v0

v1 whole, which is shorter than its diff:
```python
import jax
import jax.numpy as jnp
import numpy as np
from jax import lax
from jax.experimental import pallas as pl
from jax.experimental.pallas import tpu as pltpu
from jax.sharding import PartitionSpec as P

FF = 512
EPG = 8
MESH = pl.DeviceIdType.MESH
BVAL = (0, 1, -1, 2)
WAVE_AT = (0, 8, 24, 40, 56)
WAVE_N = (8, 16, 16, 16, 8)


def place():
    fs = lax.axis_index("fs")
    tp = lax.axis_index("tp")
    return fs // 2, fs % 2, tp // 4, tp % 4


def device(z, c, y, x):
    return {"fs": lax.rem(z + 32, 32) * 2 + c, "tp": lax.rem(y + 4, 4) * 4 + lax.rem(x + 4, 4)}


class Copies:
    def __init__(self, send, recv):
        self.send, self.recv, self.used, self.pending = send, recv, 0, []

    def slots(self, n=1):
        at = self.used
        self.used += n
        return at

    def make(self, src, dst, dev, at, to=0):
        return pltpu.make_async_remote_copy(
            src_ref=src,
            dst_ref=dst,
            send_sem=self.send.at[at],
            recv_sem=self.recv.at[at + to],
            device_id=dev,
            device_id_type=MESH,
        )

    def start(self, src, dst, dev, at, to=0, when=None):
        def go():
            self.make(src, dst, dev, at, to).start()

        def end():
            self.make(src, dst, dev, at, to).wait_send()

        if when is None:
            go()
        else:
            pl.when(when)(go)
        self.pending.append((when, end))

    def arrived(self, ref, dev, at, to=0):
        self.make(ref, ref, dev, at, to).wait_recv()

    def drain(self):
        for when, end in self.pending:
            if when is None:
                end()
            else:
                pl.when(when)(end)


def greet(partners, meanwhile=None):
    barrier = pltpu.get_barrier_semaphore()
    for dev in partners:
        pl.semaphore_signal(barrier, inc=1, device_id=dev, device_id_type=MESH)
    if meanwhile is not None:
        meanwhile()
    pl.semaphore_wait(barrier, len(partners))


def pack(gain_ref, held, s_ref, loads):
    for load in loads:
        load.start()
    eye = lax.broadcasted_iota(jnp.int32, (32, 32), 0) == lax.broadcasted_iota(jnp.int32, (32, 32), 1)
    gain = jnp.sum(jnp.where(eye, gain_ref[...], 0.0), axis=1, keepdims=True)
    hidden = lax.broadcasted_iota(jnp.int32, (32, 128), 0)
    lane = lax.broadcasted_iota(jnp.int32, (32, 128), 1)
    for n, load in enumerate(loads):
        load.wait()
        total = jnp.zeros((256, 128), jnp.float32)
        for q in range(4):
            rows = held[n, :, 8 * q : 8 * q + 8, :]
            if n < 2:
                rows = rows * gain[8 * q : 8 * q + 8][None]
            place_q = (lane == hidden + 32 * q).astype(jnp.float32).astype(jnp.bfloat16)
            total += jnp.dot(
                rows.reshape(256, 32).astype(jnp.bfloat16), place_q, preferred_element_type=jnp.float32
            )
        for e in range(32):
            s_ref[e % 4, e // 4, 8 * n : 8 * n + 8] = total[8 * e : 8 * e + 8].astype(jnp.bfloat16)


def move_kernel(
    gate_ref, up_ref, down_ref, gain_ref, f_out, held, f_ref, s_ref, abuf, bbuf, load, store, send, recv
):
    z, c, y, x = place()
    s = 1 - 2 * c
    k = z // 4
    owner = y // 2
    jy = y % 2
    rel = lax.rem(y - 2 * c + 4, 4)
    owns = rel < 2
    other = device(z, 1 - c, y, x)
    right, left = device(z, c, y, x + 1), device(z, c, y, x - 1)
    up, down = device(z, c, y + 1, x), device(z, c, y - 1, x)
    greet(
        [device(z + d, c, y, x) for d in (1, -1, 2, -2, 4, -4)]
        + [device(z + d, 1 - c, y, x) for d in (4, -4)]
        + [other, right, left, up, down],
        lambda: pack(
            gain_ref,
            held,
            s_ref,
            [
                pltpu.make_async_copy(m, held.at[n], load.at[n])
                for n, m in enumerate((gate_ref, up_ref, down_ref))
            ],
        ),
    )
    cp = Copies(send, recv)

    a_at = cp.slots(3)
    for i in (3, 1, 2):
        b = BVAL[i] * s
        cp.start(s_ref.at[lax.rem(z + b + 32, 4)], abuf.at[i], device(z + b, c, y, x), a_at + i - 1)
    abuf[0] = s_ref[lax.rem(z, 4)]
    for i in (1, 2, 3):
        cp.arrived(abuf.at[i], other, a_at + i - 1)

    def slot(a, direction):
        w = abs(a)
        if w in (0, 4):
            return WAVE_AT[w] + c * 4
        return WAVE_AT[w] + (0 if direction > 0 else 8) + c * 4

    hop = {}
    final = {}

    def stride_step(n, a):
        for side, direction in ((0, 1), (1, -1)):
            via = device(z + 4 * direction, c, y, x)
            end = device(z + 4 * direction, owner, y, x)
            half = pl.ds(2 * side, 2) if a == 4 else pl.ds(0, 4)
            width = 2 if a == 4 else 4
            if n == 1:
                src = abuf.at[half, lax.rem(k + direction * a + 8, 8)]
            else:
                src = bbuf.at[side, n - 2, a - 2, pl.ds(0, width)]
                cp.arrived(src, other, hop[side, n - 1, a])
            if a == n:
                at = cp.slots(2)
                first = slot(a, direction) + (2 * side if a == 4 else 0)
                cp.start(src, f_ref.at[jy, x, pl.ds(first, width)], end, at, c)
                final[side, a] = (at, width)
            else:
                at = cp.slots(1)
                hop[side, n, a] = at
                cp.start(src, bbuf.at[side, n - 1, a - 2, pl.ds(0, width)], via, at)

    zero_at = cp.slots(1)

    def wave_arrived(w):
        if w == 0:

            @pl.when(owns)
            def _():
                f_ref[jy, x, pl.ds(c * 4, 4)] = abuf[:, k]
                cp.arrived(f_ref.at[jy, x, pl.ds((1 - c) * 4, 4)], other, zero_at)

            return

        @pl.when(owns)
        def _():
            for side in (0, 1):
                at, width = final[side, w]
                for core in (0, 1):
                    cp.arrived(f_ref.at[jy, x, pl.ds(0, width)], other, at, core)

    ring = {}

    def ring_x(key, take, when):
        def first():
            at = ring[key] = cp.slots(4)
            cp.start(take(x, 0), take(x, 0), right, at, when=when)
            cp.start(take(x, 0), take(x, 0), left, at + 1, when=when)

        def second():
            at = ring[key]

            def wait():
                cp.arrived(take(lax.rem(x + 3, 4), 0), other, at)
                cp.arrived(take(lax.rem(x + 1, 4), 0), other, at + 1)

            if when is None:
                wait()
            else:
                pl.when(when)(wait)
            cp.start(take(lax.rem(x + 3, 4), 1), take(lax.rem(x + 3, 4), 1), right, at + 2, when=when)
            cp.start(take(lax.rem(x + 1, 4), 2), take(lax.rem(x + 1, 4), 2), left, at + 3, when=when)

        def last():
            at = ring[key]

            def wait():
                cp.arrived(take(lax.rem(x + 2, 4), 1), other, at + 2)
                cp.arrived(take(lax.rem(x + 2, 4), 2), other, at + 3)

            if when is None:
                wait()
            else:
                pl.when(when)(wait)

        return first, second, last

    plus = (rel == 1) | (rel == 2)
    minus = (rel == 0) | (rel == 3)
    got = 1 - lax.rem(rel, 2)

    def ring_y(key, take):
        def first():
            at = ring[key] = cp.slots(4)
            cp.start(take(jy, 0), take(jy, 0), up, at, when=owns)
            cp.start(take(jy, 0), take(jy, 0), down, at + 1, when=owns)

        def second():
            at = ring[key]

            @pl.when(plus)
            def _():
                cp.arrived(take(got, 0), other, at)

            @pl.when(minus)
            def _():
                cp.arrived(take(got, 0), other, at + 1)

            cp.start(take(got, 1), take(got, 1), up, at + 2, when=plus)
            cp.start(take(got, 2), take(got, 2), down, at + 3, when=minus)

        def last():
            at = ring[key]

            @pl.when(jnp.logical_not(owns))
            def _():
                cp.arrived(take(jy, 1), other, at + 2)
                cp.arrived(take(jy, 2), other, at + 3)

        return first, second, last

    def out(w):
        slots = pl.ds(WAVE_AT[w], WAVE_N[w])
        return pltpu.make_async_copy(f_ref.at[:, :, slots], f_out.at[:, :, slots], store.at[w])

    def wave(w):
        n = WAVE_N[w] // 2
        h1, h2 = WAVE_AT[w], WAVE_AT[w] + n

        def part(base, p):
            return pl.ds(base, n) if p == 0 else pl.ds(base + (p - 1) * (n // 2), n // 2)

        x1, x2, x3 = ring_x((w, 0), lambda i, p: f_ref.at[jy, i, part(h1, p)], owns)
        y1, y2, y3 = ring_y((w, 1), lambda j, p: f_ref.at[j, :, part(h1, p)])
        v1, v2, v3 = ring_y((w, 2), lambda j, p: f_ref.at[j, x, part(h2, p)])
        u1, u2, u3 = ring_x((w, 3), lambda i, p: f_ref.at[:, i, part(h2, p)], None)

        def t0():
            wave_arrived(w)
            x1()
            v1()

        def t1():
            x2()
            v2()

        def t2():
            x3()
            v3()
            y1()
            u1()

        def t3():
            y2()
            u2()

        def t4():
            y3()
            u3()
            out(w).start()

        return t0, t1, t2, t3, t4

    for a in (4, 3, 2, 1):
        stride_step(1, a)
    cp.start(
        abuf.at[:, k], f_ref.at[jy, x, pl.ds(c * 4, 4)], other, zero_at, when=jnp.logical_not(owns)
    )
    ticks = [wave(w) for w in range(5)]
    for kind, n, m in SCHEDULE:
        if kind == "B":
            stride_step(int(n), int(m))
        else:
            ticks[int(n)][int(m)]()
    for w in range(5):
        out(w).wait()
    cp.drain()
    assert cp.used <= SEMS, cp.used


SCHEDULE = (
    ("w00", "B24", "B23", "B22", "w10", "w01", "B34")
    + ("B33", "w20", "w11", "w02", "B44", "w30", "w21", "w12", "w03")
    + ("w40", "w31", "w22", "w13", "w04", "w41", "w32", "w23", "w14")
    + ("w42", "w33", "w24", "w43", "w34", "w44")
)
SEMS = 120


def move(gate, up, down, gain):
    return pl.pallas_call(
        move_kernel,
        out_shape=jax.ShapeDtypeStruct((2, 4, 64, 24, 128), jnp.bfloat16),
        in_specs=[pl.BlockSpec(memory_space=pl.ANY)] * 3 + [pl.BlockSpec(memory_space=pltpu.VMEM)],
        out_specs=pl.BlockSpec(memory_space=pl.ANY),
        scratch_shapes=[
            pltpu.VMEM((3, 32, 32, 32), jnp.float32),
            pltpu.VMEM((2, 4, 64, 24, 128), jnp.bfloat16),
            pltpu.VMEM((4, 8, 24, 128), jnp.bfloat16),
            pltpu.VMEM((4, 8, 24, 128), jnp.bfloat16),
            pltpu.VMEM((2, 3, 3, 4, 24, 128), jnp.bfloat16),
            pltpu.SemaphoreType.DMA((3,)),
            pltpu.SemaphoreType.DMA((5,)),
            pltpu.SemaphoreType.DMA((SEMS,)),
            pltpu.SemaphoreType.DMA((SEMS,)),
        ],
        compiler_params=pltpu.CompilerParams(
            collective_id=0, has_side_effects=True, vmem_limit_bytes=56 << 20
        ),
    )(gate, up, down, gain)


def expert_kernel(
    f_hbm,
    prompt_ref,
    group_ref,
    inner_ref,
    weight_ref,
    turn_ref,
    gate_out,
    up_out,
    down_out,
    part_ref,
    f_ref,
    normed,
    gate_ref,
    up_ref,
    down_ref,
    load,
    sems,
):
    z = lax.axis_index("fs") // 2

    def fetch(w):
        slots = pl.ds(WAVE_AT[w], WAVE_N[w])
        return pltpu.make_async_copy(f_hbm.at[:, :, slots], f_ref.at[:, :, slots], load.at[w])

    for w in range(5):
        fetch(w).start()
    values = prompt_ref[...].astype(jnp.float32)
    normed[...] = (
        values * lax.rsqrt(jnp.mean(values * values, axis=1, keepdims=True) + 1e-06)
    ).astype(jnp.bfloat16)
    for w in range(5):
        fetch(w).wait()
        for j in (0, 1):
            at, n = WAVE_AT[w], WAVE_N[w]
            taken = [
                f_ref[j, i, at : at + n].astype(jnp.float32).reshape(n * 24, 128).astype(jnp.bfloat16)
                for i in range(4)
            ]
            turned = jnp.dot(
                jnp.concatenate(taken, axis=1), turn_ref[...], preferred_element_type=jnp.float32
            )
            for m in range(n):
                side, core, b, a = slot_source(w, m)
                source = lax.rem(z - 4 * a - (1 - 2 * core) * BVAL[b] + 64, 32)
                row = pl.multiple_of((source * 2 + core) * 32, 32)
                for k, out in enumerate((gate_ref, up_ref, down_ref)):
                    first = m * 24 + k * 8
                    rows = [turned[first : first + 8, 128 * q : 128 * q + 128] for q in range(4)]
                    out[pl.ds(row, 32), 128 * j : 128 * j + 128] = jnp.concatenate(
                        rows, axis=0
                    ).astype(jnp.bfloat16)
    stores = [
        pltpu.make_async_copy(a, b, sems.at[i])
        for i, (a, b) in enumerate(((gate_ref, gate_out), (up_ref, up_out), (down_ref, down_out)))
    ]
    for store in stores:
        store.start()
    gate_act = jnp.dot(normed[...], gate_ref[...], preferred_element_type=jnp.float32) * 2048 ** (-0.5)
    up_act = jnp.dot(normed[...], up_ref[...], preferred_element_type=jnp.float32) * 2048 ** (-0.5)
    chosen = group_ref[...] * EPG + inner_ref[...]
    row = jnp.sum(jnp.where(chosen == z, weight_ref[...], 0.0), axis=0, keepdims=True)
    column = jnp.broadcast_to(row, (8, 256)).T[:, :1]
    silu = gate_act / (1.0 + jnp.exp(-gate_act))
    scaled = (column * silu * up_act).astype(jnp.bfloat16)
    for n in range(8):
        part = lax.dot_general(
            down_ref[n * 256 : (n + 1) * 256],
            scaled,
            (((1,), (1,)), ((), ())),
            preferred_element_type=jnp.float32,
        ).astype(jnp.bfloat16)
        for i in range(8):
            owner = n * 8 + i
            part_ref[owner % 2, owner // 2 % 4, owner // 8] = part[i * 32 : (i + 1) * 32]
    for store in stores:
        store.wait()


def slot_source(w, m):
    if w in (0, 4):
        return 0, m // 4, m % 4, w
    side, rest = divmod(m, 8)
    return side, rest // 4, rest % 4, -w if side else w


EXPERT_VMEM = 51


def turning():
    at = np.arange(512).reshape(4, 4, 32).transpose(1, 0, 2).reshape(512)
    return np.eye(512, dtype=np.float32)[:, at]


def expert(moved, prompt, group, inner, weight):
    served = jax.ShapeDtypeStruct((2048, 256), jnp.bfloat16)
    vmem = pl.BlockSpec(memory_space=pltpu.VMEM)
    hbm = pl.BlockSpec(memory_space=pl.ANY)
    return pl.pallas_call(
        expert_kernel,
        out_shape=(served, served, served, jax.ShapeDtypeStruct((2, 4, 8, 32, 256), jnp.bfloat16)),
        in_specs=[hbm] + [vmem] * 5,
        out_specs=(hbm, hbm, hbm, vmem),
        scratch_shapes=[
            pltpu.VMEM((2, 4, 64, 24, 128), jnp.bfloat16),
            pltpu.VMEM((256, 2048), jnp.bfloat16),
            pltpu.VMEM((2048, 256), jnp.bfloat16),
            pltpu.VMEM((2048, 256), jnp.bfloat16),
            pltpu.VMEM((2048, 256), jnp.bfloat16),
            pltpu.SemaphoreType.DMA((5,)),
            pltpu.SemaphoreType.DMA((3,)),
        ],
        compiler_params=pltpu.CompilerParams(vmem_limit_bytes=EXPERT_VMEM << 20),
    )(moved, prompt, group, inner, weight, jnp.asarray(turning(), jnp.bfloat16))


FAR_FIRST = (4, 3, -3, 2, -2, 1, -1, 0)


def sum_kernel(p_ref, o_ref, xbuf, qbuf, abuf, ubuf, rbuf, tbuf, send, recv):
    z, c, y, x = place()
    s = 1 - 2 * c
    k = z // 4
    other = device(z, 1 - c, y, x)
    greet([device(z + d, c, y, x) for d in (1, -1, 2, -2, 4, -4)] + [other])
    cp = Copies(send, recv)

    def chunk(near, a):
        near = lax.rem(near + 32, 32)
        return lax.rem(near, 4), lax.rem(near // 4 + a + 8, 8)

    order = (3, 1, 2, 0)
    core_at = {}
    for a in FAR_FIRST:
        for i in order:
            q, at = chunk(z - BVAL[i] * s, a)
            core_at[a, i] = cp.slots()
            cp.start(p_ref.at[1 - c, q, at], xbuf.at[q, at], other, core_at[a, i])
    near_at = {}
    for a in FAR_FIRST:
        for i in order:
            q, at = chunk(z + BVAL[i] * s, a)
            cp.arrived(xbuf.at[q, at], other, core_at[a, i])
            n = (a + 8) % 8
            total = p_ref[c, q, at].astype(jnp.float32) + xbuf[q, at].astype(jnp.float32)
            qbuf[i, n] = total.astype(jnp.bfloat16)
            if i:
                near_at[a, i] = cp.slots()
                cp.start(
                    qbuf.at[i, n], abuf.at[i - 1, n], device(z + BVAL[i] * s, c, y, x), near_at[a, i]
                )

    def mine(a):
        at = (a + 8) % 8
        for i in (1, 2, 3):
            cp.arrived(abuf.at[i - 1, at], other, near_at[a, i])
        total = qbuf[0, at].astype(jnp.float32) + abuf[0, at].astype(jnp.float32)
        return total + (abuf[1, at].astype(jnp.float32) + abuf[2, at].astype(jnp.float32))

    via = (device(z + 4, c, y, x), device(z - 4, c, y, x))
    ring_at = [cp.slots(2) for _ in range(4)]
    ubuf[...] = mine(4).astype(jnp.bfloat16)
    for side in (0, 1):
        rows = pl.ds(16 * side, 16)
        cp.start(ubuf.at[rows], rbuf.at[side, 0, rows], via[side], ring_at[0] + side)
    for n in (1, 2, 3):
        held = [mine(4 - n), mine(n - 4)]
        for side in (0, 1):
            if n == 1:
                rows = pl.ds(16 * side, 16)
                cp.arrived(rbuf.at[side, 0, rows], other, ring_at[0] + side)
                came = rbuf[side, 0, 16 * side : 16 * side + 16].astype(jnp.float32)
                tbuf[side, 0, 16 * side : 16 * side + 16] = (
                    held[side][16 * side : 16 * side + 16] + came
                ).astype(jnp.bfloat16)
                tbuf[side, 0, 16 - 16 * side : 32 - 16 * side] = held[side][
                    16 - 16 * side : 32 - 16 * side
                ].astype(jnp.bfloat16)
            else:
                cp.arrived(rbuf.at[side, n - 1], other, ring_at[n - 1] + side)
                tbuf[side, n - 1] = (held[side] + rbuf[side, n - 1].astype(jnp.float32)).astype(
                    jnp.bfloat16
                )
            cp.start(tbuf.at[side, n - 1], rbuf.at[side, n], via[side], ring_at[n] + side)
    total = mine(0)
    for side in (0, 1):
        cp.arrived(rbuf.at[side, 3], other, ring_at[3] + side)
        total = total + rbuf[side, 3].astype(jnp.float32)
    o_ref[...] = (total * FF ** (-0.5)).astype(jnp.bfloat16)
    cp.drain()


def summed(parts):
    return pl.pallas_call(
        sum_kernel,
        out_shape=jax.ShapeDtypeStruct((32, 256), jnp.bfloat16),
        in_specs=[pl.BlockSpec(memory_space=pltpu.VMEM)],
        out_specs=pl.BlockSpec(memory_space=pltpu.VMEM),
        scratch_shapes=[
            pltpu.VMEM((4, 8, 32, 256), jnp.bfloat16),
            pltpu.VMEM((4, 8, 32, 256), jnp.bfloat16),
            pltpu.VMEM((3, 8, 32, 256), jnp.bfloat16),
            pltpu.VMEM((32, 256), jnp.bfloat16),
            pltpu.VMEM((2, 4, 32, 256), jnp.bfloat16),
            pltpu.VMEM((2, 3, 32, 256), jnp.bfloat16),
            pltpu.SemaphoreType.DMA((64,)),
            pltpu.SemaphoreType.DMA((64,)),
        ],
        compiler_params=pltpu.CompilerParams(
            collective_id=1, has_side_effects=True, vmem_limit_bytes=16 << 20
        ),
    )(parts)


def shards(
    prompt, norm_gain, gate_master, up_master, down_master, group_choice, inner_choice, route_weight
):
    moved = move(gate_master, up_master, down_master, norm_gain[None, :])
    gate, up, down, parts = expert(
        moved, prompt, group_choice[None, :], inner_choice.T, route_weight.T
    )
    return gate, up, down, summed(parts).T


def solution(mesh):
    in_specs = (
        P("tp", None),
        P("fs"),
        P(None, "fs", "tp"),
        P(None, "fs", "tp"),
        P(None, "fs", "tp"),
        P("tp"),
        P("tp", None),
        P("tp", None),
    )
    out_specs = (P(None, "fs"), P(None, "fs"), P(None, "fs"), P("tp", "fs"))
    return jax.shard_map(
        shards, mesh=mesh, in_specs=in_specs, out_specs=out_specs, check_vma=False
    )
```

time: 328 us -> 107 us (0.33)
  the two profiles are of different devices: /device:TPU:4 before, /device:TPU:1 now
where the time goes in v1:
time: 107 us; the launch traced here: 105 us
  Pallas kernels  104 us (97%)
    pallas_call x1, Pallas kernels, move(): pl.pallas_call(move_kernel, out_shape=jax.ShapeDtypeStruct((2, 4, 64, 24,...  69.1 us
    pallas_call x1, Pallas kernels, summed(): pl.pallas_call(sum_kernel, out_shape=jax.ShapeDtypeStruct((32, 256), jnp....  29.2 us
    pallas_call x1, Pallas kernels, expert(): pl.pallas_call(expert_kernel, out_shape=(served, served, served, jax.Shap...  5.67 us

profile of v1, /device:TPU:1, one launch (start us, length us, event | category | flops | bytes accessed | tf_op | source)
XLA Modules:
  0.0 105.3 jit_solution(15434459323912859959)
XLA Ops:
  0.6 0.0 copy-start.1
  0.6 0.0 copy-start.3
  0.7 0.0 copy-start.2
  0.7 0.0 copy-start.4
  0.7 0.0 copy-start
  0.7 69.1 %shard_map.120.f_hbm = bf16[2,4,64,24,128]{4,3,2,1,0:T(8,128)(2,1)} custom-call(f32[32,32,32]{2,1,0:T(8,128)} %gate_ref.1, f32[32,32,32]{2,1,0:T(8,128)} %up_ref.1, f32[32,32,32]{2,1,0:T(8,128)} %down_ref.1, f32[1,32]{1,0:T(1,128)} %bitcast.9), custom_call_target="tpu_custom_call" | custom-call | tf_op jit(solution)/shard_map/pallas_call | solution.py:326
  69.8 0.0 copy-done.1
  69.8 0.0 copy-done.3
  69.8 0.0 copy-done.2
  69.8 0.0 copy-done.4
  69.8 0.0 copy-done
  69.8 5.7 %shard_map.121 = (bf16[2048,256]{1,0:T(8,128)(2,1)}, bf16[2048,256]{1,0:T(8,128)(2,1)}, bf16[2048,256]{1,0:T(8,128)(2,1)}, bf16[2,4,8,32,256]{4,3,2,1,0:T(8,128)(2,1)S(1)}) custom-call(bf16[2,4,64,24,128]{4,3,2,1,0:T(8,128)(2,1)} %shard_map.120.f_hbm, bf16[256,2048]{1,0:T(8,128)(2,1)S(1)} %copy-done, s32[1,256]{1,0:T(1,128)S(1)} %bitcast.8, ...), custom_call_target="tpu_custom_call" | custom-call | tf_op jit(solution)/shard_map/pallas_call | solution.py:446
  75.5 29.2 %shard_map.122 = bf16[32,256]{1,0:T(8,128)(2,1)S(1)} custom-call(bf16[2,4,8,32,256]{4,3,2,1,0:T(8,128)(2,1)S(1)} %get-tuple-element.11.p_ref), custom_call_target="tpu_custom_call" | custom-call | tf_op jit(solution)/shard_map/pallas_call | solution.py:541
  104.7 0.6 copy.14
Async XLA Ops:
  0.6 69.2 %copy-start.1 = (bf16[512,512]{1,0:T(8,128)(2,1)S(1)}, bf16[512,512]{1,0:T(8,128)(2,1)}, u32[]{:S(2)}) copy-start(bf16[512,512]{1,0:T(8,128)(2,1)} %constant.2.clone.turn_ref) | copy-start | bytes 1572868
  0.6 69.2 %copy-start.3 = (f32[256,2]{0,1:T(2,128)S(1)}, f32[256,2]{0,1:T(2,128)}, u32[]{:S(2)}) copy-start(f32[256,2]{0,1:T(2,128)} %param.16) | copy-start | bytes 6148
  0.7 69.2 %copy-start.2 = (s32[256,2]{0,1:T(2,128)S(1)}, s32[256,2]{0,1:T(2,128)}, u32[]{:S(2)}) copy-start(s32[256,2]{0,1:T(2,128)} %param.15) | copy-start | bytes 6148
  0.7 69.2 %copy-start.4 = (s32[256]{0:T(256)S(1)}, s32[256]{0:T(256)}, u32[]{:S(2)}) copy-start(s32[256]{0:T(256)} %param.14) | copy-start | bytes 3076
  0.7 69.2 %copy-start = (bf16[256,2048]{1,0:T(8,128)(2,1)S(1)}, bf16[256,2048]{1,0:T(8,128)(2,1)}, u32[]{:S(2)}) copy-start(bf16[256,2048]{1,0:T(8,128)(2,1)} %prompt_ref.1) | copy-start | bytes 3145732

commit v2 on v1

v2 whole, which is shorter than its diff:
```python
import jax
import jax.numpy as jnp
import numpy as np
from jax import lax
from jax.experimental import pallas as pl
from jax.experimental.pallas import tpu as pltpu
from jax.sharding import PartitionSpec as P

FF = 512
EPG = 8
MESH = pl.DeviceIdType.MESH
BVAL = (0, 1, -1, 2)
WAVE_AT = (0, 8, 24, 40, 56)
WAVE_N = (8, 16, 16, 16, 8)
FAR_FIRST = (4, 3, -3, 2, -2, 1, -1, 0)


def place():
    fs = lax.axis_index("fs")
    tp = lax.axis_index("tp")
    return fs // 2, fs % 2, tp // 4, tp % 4


def device(z, c, y, x):
    return {"fs": lax.rem(z + 32, 32) * 2 + c, "tp": lax.rem(y + 4, 4) * 4 + lax.rem(x + 4, 4)}


def chunk(near, a):
    near = lax.rem(near + 32, 32)
    return lax.rem(near, 4), lax.rem(near // 4 + a + 8, 8)


class Copies:
    def __init__(self, send, recv):
        self.send, self.recv, self.used, self.pending = send, recv, 0, []

    def slots(self, n=1):
        at = self.used
        self.used += n
        return at

    def make(self, src, dst, dev, at, to=0):
        return pltpu.make_async_remote_copy(
            src_ref=src,
            dst_ref=dst,
            send_sem=self.send.at[at],
            recv_sem=self.recv.at[at + to],
            device_id=dev,
            device_id_type=MESH,
        )

    def start(self, src, dst, dev, at, to=0, when=None):
        def go():
            self.make(src, dst, dev, at, to).start()

        def end():
            self.make(src, dst, dev, at, to).wait_send()

        if when is None:
            go()
        else:
            pl.when(when)(go)
        self.pending.append((when, end))

    def arrived(self, ref, dev, at, to=0):
        self.make(ref, ref, dev, at, to).wait_recv()

    def drain(self):
        for when, end in self.pending:
            if when is None:
                end()
            else:
                pl.when(when)(end)


def greet(partners, meanwhile=None):
    barrier = pltpu.get_barrier_semaphore()
    for dev in partners:
        pl.semaphore_signal(barrier, inc=1, device_id=dev, device_id_type=MESH)
    if meanwhile is not None:
        meanwhile()
    pl.semaphore_wait(barrier, len(partners))


def pack(gain_ref, held, s_ref, gain_load, loads):
    gain_load.wait()
    eye = lax.broadcasted_iota(jnp.int32, (32, 32), 0) == lax.broadcasted_iota(jnp.int32, (32, 32), 1)
    gain = jnp.sum(jnp.where(eye, gain_ref[...], 0.0), axis=1, keepdims=True)
    hidden = lax.broadcasted_iota(jnp.int32, (32, 128), 0)
    lane = lax.broadcasted_iota(jnp.int32, (32, 128), 1)
    for n, load in enumerate(loads):
        load.wait()
        total = jnp.zeros((256, 128), jnp.float32)
        for q in range(4):
            rows = held[n, :, 8 * q : 8 * q + 8, :]
            if n < 2:
                rows = rows * gain[8 * q : 8 * q + 8][None]
            place_q = (lane == hidden + 32 * q).astype(jnp.float32).astype(jnp.bfloat16)
            total += jnp.dot(
                rows.reshape(256, 32).astype(jnp.bfloat16), place_q, preferred_element_type=jnp.float32
            )
        for e in range(32):
            s_ref[e % 4, e // 4, 8 * n : 8 * n + 8] = total[8 * e : 8 * e + 8].astype(jnp.bfloat16)


def partners():
    z, c, y, x = place()
    near = [device(z + d, c, y, x) for d in (1, -1, 2, -2, 4, -4)]
    near += [device(z + d, 1 - c, y, x) for d in (4, -4)] + [device(z, 1 - c, y, x)]
    flat = ((0, 1), (0, -1), (1, 0), (-1, 0), (0, 2), (2, 0))
    return near + [device(z, c, y + b, x + a) for b, a in flat]


def move(cp, s_ref, abuf, bbuf, f_ref, settle, meanwhile):
    z, c, y, x = place()
    s = 1 - 2 * c
    owner = y // 2
    jy = y % 2
    rel = lax.rem(y - 2 * c + 4, 4)
    owns = rel < 2
    other = device(z, 1 - c, y, x)
    right, left = device(z, c, y, x + 1), device(z, c, y, x - 1)
    up, down = device(z, c, y + 1, x), device(z, c, y - 1, x)

    near_at = {}
    for a in FAR_FIRST:
        for i in (3, 1, 2):
            near = z + BVAL[i] * s
            q, at = chunk(near, a)
            near_at[a, i] = cp.slots()
            cp.start(s_ref.at[q, at], abuf.at[i, (a + 8) % 8], device(near, c, y, x), near_at[a, i])
    for a in FAR_FIRST:
        q, at = chunk(z, a)
        abuf[0, (a + 8) % 8] = s_ref[q, at]

    meanwhile()

    def near_arrived(a):
        for i in (1, 2, 3):
            cp.arrived(abuf.at[i, (a + 8) % 8], other, near_at[a, i])

    def slot(a, direction):
        w = abs(a)
        if w in (0, 4):
            return WAVE_AT[w] + c * 4
        return WAVE_AT[w] + (0 if direction > 0 else 8) + c * 4

    hop = {}
    final = {}

    def stride_step(n, a):
        for side, direction in ((0, 1), (1, -1)):
            via = device(z + 4 * direction, c, y, x)
            end = device(z + 4 * direction, owner, y, x)
            half = pl.ds(2 * side, 2) if a == 4 else pl.ds(0, 4)
            width = 2 if a == 4 else 4
            if n == 1:
                src = abuf.at[half, (direction * a + 8) % 8]
            else:
                src = bbuf.at[side, n - 2, a - 2, pl.ds(0, width)]
                cp.arrived(src, other, hop[side, n - 1, a])
            if a == n:
                at = cp.slots(2)
                first = slot(a, direction) + (2 * side if a == 4 else 0)
                cp.start(src, f_ref.at[jy, x, pl.ds(first, width)], end, at, c)
                final[side, a] = (at, width)
            else:
                at = cp.slots(1)
                hop[side, n, a] = at
                cp.start(src, bbuf.at[side, n - 1, a - 2, pl.ds(0, width)], via, at)

    zero_at = cp.slots(1)

    def wave_arrived(w):
        if w == 0:

            @pl.when(owns)
            def _():
                f_ref[jy, x, pl.ds(c * 4, 4)] = abuf[:, 0]
                cp.arrived(f_ref.at[jy, x, pl.ds((1 - c) * 4, 4)], other, zero_at)

            return

        @pl.when(owns)
        def _():
            for side in (0, 1):
                at, width = final[side, w]
                for core in (0, 1):
                    cp.arrived(f_ref.at[jy, x, pl.ds(0, width)], other, at, core)

    ring = {}

    def direct_x(key, take, when):
        def first():
            at = ring[key] = cp.slots(3)
            for n, d in enumerate((2, 1, 3)):
                cp.start(take(x, 0), take(x, 0), device(z, c, y, x + d), at + n, when=when)

        def second():
            def wait():
                for n, d in enumerate((2, 1, 3)):
                    cp.arrived(take(lax.rem(x + 4 - d, 4), 0), other, ring[key] + n)

            if when is None:
                wait()
            else:
                pl.when(when)(wait)

        return first, second

    def direct_y(key, take):
        def first():
            at = ring[key] = cp.slots(3)
            for n, d in enumerate((2, 1, 3)):
                cp.start(take(jy, 0), take(jy, 0), device(z, c, y + d, x), at + n, when=owns)

        def second():
            at = ring[key]

            @pl.when(plus)
            def _():
                cp.arrived(take(got, 0), other, at + 1)

            @pl.when(minus)
            def _():
                cp.arrived(take(got, 0), other, at + 2)

            @pl.when(jnp.logical_not(owns))
            def _():
                cp.arrived(take(jy, 0), other, at)

        return first, second

    def ring_x(key, take, when):
        def first():
            at = ring[key] = cp.slots(4)
            cp.start(take(x, 0), take(x, 0), right, at, when=when)
            cp.start(take(x, 0), take(x, 0), left, at + 1, when=when)

        def second():
            at = ring[key]

            def wait():
                cp.arrived(take(lax.rem(x + 3, 4), 0), other, at)
                cp.arrived(take(lax.rem(x + 1, 4), 0), other, at + 1)

            if when is None:
                wait()
            else:
                pl.when(when)(wait)
            cp.start(take(lax.rem(x + 3, 4), 1), take(lax.rem(x + 3, 4), 1), right, at + 2, when=when)
            cp.start(take(lax.rem(x + 1, 4), 2), take(lax.rem(x + 1, 4), 2), left, at + 3, when=when)

        def last():
            at = ring[key]

            def wait():
                cp.arrived(take(lax.rem(x + 2, 4), 1), other, at + 2)
                cp.arrived(take(lax.rem(x + 2, 4), 2), other, at + 3)

            if when is None:
                wait()
            else:
                pl.when(when)(wait)

        return first, second, last

    plus = (rel == 1) | (rel == 2)
    minus = (rel == 0) | (rel == 3)
    got = 1 - lax.rem(rel, 2)

    def ring_y(key, take):
        def first():
            at = ring[key] = cp.slots(4)
            cp.start(take(jy, 0), take(jy, 0), up, at, when=owns)
            cp.start(take(jy, 0), take(jy, 0), down, at + 1, when=owns)

        def second():
            at = ring[key]

            @pl.when(plus)
            def _():
                cp.arrived(take(got, 0), other, at)

            @pl.when(minus)
            def _():
                cp.arrived(take(got, 0), other, at + 1)

            cp.start(take(got, 1), take(got, 1), up, at + 2, when=plus)
            cp.start(take(got, 2), take(got, 2), down, at + 3, when=minus)

        def last():
            at = ring[key]

            @pl.when(jnp.logical_not(owns))
            def _():
                cp.arrived(take(jy, 1), other, at + 2)
                cp.arrived(take(jy, 2), other, at + 3)

        return first, second, last

    def wave(w):
        n = WAVE_N[w] // 2
        h1, h2 = WAVE_AT[w], WAVE_AT[w] + n

        def part(base, p):
            return pl.ds(base, n) if p == 0 else pl.ds(base + (p - 1) * (n // 2), n // 2)

        views = (
            lambda i, p: f_ref.at[jy, i, part(h1, p)],
            lambda j, p: f_ref.at[j, :, part(h1, p)],
            lambda j, p: f_ref.at[j, x, part(h2, p)],
            lambda i, p: f_ref.at[:, i, part(h2, p)],
        )
        if w in DIRECT:
            x1, x2 = direct_x((w, 0), views[0], owns)
            y1, y2 = direct_y((w, 1), views[1])
            v1, v2 = direct_y((w, 2), views[2])
            u1, u2 = direct_x((w, 3), views[3], None)

            def d0():
                wave_arrived(w)
                x1()
                v1()

            def d1():
                x2()
                y1()
                v2()
                u1()

            def d2():
                y2()
                u2()
                settle(w)

            return d0, d1, d2
        x1, x2, x3 = ring_x((w, 0), views[0], owns)
        y1, y2, y3 = ring_y((w, 1), views[1])
        v1, v2, v3 = ring_y((w, 2), views[2])
        u1, u2, u3 = ring_x((w, 3), views[3], None)

        def t0():
            wave_arrived(w)
            x1()
            v1()

        def t1():
            x2()
            v2()

        def t2():
            x3()
            v3()
            y1()
            u1()

        def t3():
            y2()
            u2()

        def t4():
            y3()
            u3()
            settle(w)

        return t0, t1, t2, t3, t4

    for a in (4, 3, 2, 1):
        near_arrived(a)
        if a < 4:
            near_arrived(-a)
        stride_step(1, a)
    near_arrived(0)
    cp.start(
        abuf.at[:, 0], f_ref.at[jy, x, pl.ds(c * 4, 4)], other, zero_at, when=jnp.logical_not(owns)
    )
    ticks = [wave(w) for w in range(5)]
    for kind, n, m in SCHEDULE:
        if kind == "B":
            stride_step(int(n), int(m))
        else:
            ticks[int(n)][int(m)]()


DIRECT = (4,)
SCHEDULE = (
    ("w00", "B24", "B23", "B22", "w10", "w01", "B34")
    + ("B33", "w20", "w11", "w02", "B44", "w30", "w21", "w12", "w03")
    + ("w40", "w31", "w22", "w13", "w04", "w41", "w32", "w23", "w14")
    + ("w42", "w33", "w24", "w34")
)
SEMS = 208


def slot_source(w, m):
    if w in (0, 4):
        return 0, m // 4, m % 4, w
    side, rest = divmod(m, 8)
    return side, rest // 4, rest % 4, -w if side else w


def turning():
    at = np.arange(512).reshape(4, 4, 32).transpose(1, 0, 2).reshape(512)
    return np.eye(512, dtype=np.float32)[:, at]


def settle_wave(w, z, f_ref, turn_ref, served):
    at, n = WAVE_AT[w], WAVE_N[w]
    for j in (0, 1):
        taken = [
            f_ref[j, i, at : at + n].astype(jnp.float32).reshape(n * 24, 128).astype(jnp.bfloat16)
            for i in range(4)
        ]
        turned = jnp.dot(
            jnp.concatenate(taken, axis=1), turn_ref[...], preferred_element_type=jnp.float32
        )
        for m in range(n):
            side, core, b, a = slot_source(w, m)
            source = lax.rem(z - 4 * a - (1 - 2 * core) * BVAL[b] + 64, 32)
            row = pl.multiple_of((source * 2 + core) * 32, 32)
            for k in range(3):
                first = m * 24 + k * 8
                rows = [turned[first : first + 8, 128 * q : 128 * q + 128] for q in range(4)]
                served[k, pl.ds(row, 32), 128 * j : 128 * j + 128] = jnp.concatenate(
                    rows, axis=0
                ).astype(jnp.bfloat16)


def partial_sums(z, normed, served, group_ref, inner_ref, weight_ref, part_ref):
    gate_act = jnp.dot(normed[...], served[0], preferred_element_type=jnp.float32) * 2048 ** (-0.5)
    up_act = jnp.dot(normed[...], served[1], preferred_element_type=jnp.float32) * 2048 ** (-0.5)
    chosen = group_ref[...] * EPG + inner_ref[...]
    row = jnp.sum(jnp.where(chosen == z, weight_ref[...], 0.0), axis=0, keepdims=True)
    column = jnp.broadcast_to(row, (8, 256)).T[:, :1]
    silu = gate_act / (1.0 + jnp.exp(-gate_act))
    scaled = (column * silu * up_act).astype(jnp.bfloat16)
    for n in range(8):
        part = lax.dot_general(
            served[2, n * 256 : (n + 1) * 256],
            scaled,
            (((1,), (1,)), ((), ())),
            preferred_element_type=jnp.float32,
        ).astype(jnp.bfloat16)
        for i in range(8):
            owner = n * 8 + i
            part_ref[owner % 2, owner // 2 % 4, owner // 8] = part[i * 32 : (i + 1) * 32]


def sum_parts(cp, p_ref, o_ref, xbuf, qbuf, abuf, ubuf, rbuf, tbuf):
    z, c, y, x = place()
    s = 1 - 2 * c
    other = device(z, 1 - c, y, x)
    order = (3, 1, 2, 0)
    core_at = {}
    for a in FAR_FIRST:
        for i in order:
            q, at = chunk(z - BVAL[i] * s, a)
            core_at[a, i] = cp.slots()
            cp.start(p_ref.at[1 - c, q, at], xbuf.at[q, at], other, core_at[a, i])
    near_at = {}
    for a in FAR_FIRST:
        for i in order:
            q, at = chunk(z + BVAL[i] * s, a)
            cp.arrived(xbuf.at[q, at], other, core_at[a, i])
            n = (a + 8) % 8
            total = p_ref[c, q, at].astype(jnp.float32) + xbuf[q, at].astype(jnp.float32)
            qbuf[i, n] = total.astype(jnp.bfloat16)
            if i:
                near_at[a, i] = cp.slots()
                cp.start(
                    qbuf.at[i, n], abuf.at[i - 1, n], device(z + BVAL[i] * s, c, y, x), near_at[a, i]
                )

    def mine(a):
        at = (a + 8) % 8
        for i in (1, 2, 3):
            cp.arrived(abuf.at[i - 1, at], other, near_at[a, i])
        total = qbuf[0, at].astype(jnp.float32) + abuf[0, at].astype(jnp.float32)
        return total + (abuf[1, at].astype(jnp.float32) + abuf[2, at].astype(jnp.float32))

    via = (device(z + 4, c, y, x), device(z - 4, c, y, x))
    ring_at = [cp.slots(4) for _ in range(4)]

    def onward(n, side, h, source):
        rows = pl.ds(16 * h, 16)
        cp.start(source, rbuf.at[side, n, rows], via[side], ring_at[n] + 2 * side + h)

    def came(n, side, h):
        rows = pl.ds(16 * h, 16)
        cp.arrived(rbuf.at[side, n, rows], other, ring_at[n] + 2 * side + h)
        return rbuf[side, n, 16 * h : 16 * h + 16].astype(jnp.float32)

    ubuf[...] = mine(4).astype(jnp.bfloat16)
    for side in (0, 1):
        onward(0, side, side, ubuf.at[pl.ds(16 * side, 16)])
    for n in (1, 2, 3):
        held = [mine(4 - n), mine(n - 4)]
        for order in (0, 1):
            for side in (0, 1):
                h = side if order == (0 if n > 1 else 1) else 1 - side
                total = held[side][16 * h : 16 * h + 16]
                if n > 1 or h == side:
                    total = total + came(n - 1, side, h)
                tbuf[side, n - 1, 16 * h : 16 * h + 16] = total.astype(jnp.bfloat16)
                onward(n, side, h, tbuf.at[side, n - 1, pl.ds(16 * h, 16)])
    total = mine(0)
    sums = [
        total[16 * h : 16 * h + 16] + came(3, h, h) + came(3, 1 - h, h) for h in (0, 1)
    ]
    total = jnp.concatenate(sums, axis=0)
    o_ref[...] = (total * FF ** (-0.5)).astype(jnp.bfloat16)


def whole_kernel(
    gate_hbm,
    up_hbm,
    down_hbm,
    gain_hbm,
    prompt_hbm,
    group_hbm,
    inner_hbm,
    weight_hbm,
    turn_hbm,
    gate_out,
    up_out,
    down_out,
    o_ref,
    held,
    gain,
    prompt,
    group,
    inner,
    weight,
    turn,
    s_ref,
    abuf,
    bbuf,
    f_ref,
    normed,
    served,
    part,
    xbuf,
    qbuf,
    nbuf,
    ubuf,
    rbuf,
    tbuf,
    load,
    store,
    send,
    recv,
):
    z = lax.axis_index("fs") // 2
    pairs = (
        (gain_hbm, gain),
        (gate_hbm, held.at[0]),
        (up_hbm, held.at[1]),
        (down_hbm, held.at[2]),
        (prompt_hbm, prompt),
        (turn_hbm, turn),
        (group_hbm, group),
        (inner_hbm, inner),
        (weight_hbm, weight),
    )
    loads = [pltpu.make_async_copy(a, b, load.at[n]) for n, (a, b) in enumerate(pairs)]
    stores = [
        pltpu.make_async_copy(served.at[n], out, store.at[n])
        for n, out in enumerate((gate_out, up_out, down_out))
    ]

    def ready():
        for copy in loads:
            copy.start()
        pack(gain, held, s_ref, loads[0], loads[1:4])

    def meanwhile():
        for copy in loads[4:]:
            copy.wait()
        values = prompt[...].astype(jnp.float32)
        normed[...] = (
            values * lax.rsqrt(jnp.mean(values * values, axis=1, keepdims=True) + 1e-06)
        ).astype(jnp.bfloat16)

    greet(partners(), ready)
    cp = Copies(send, recv)
    move(
        cp, s_ref, abuf, bbuf, f_ref, lambda w: settle_wave(w, z, f_ref, turn, served), meanwhile
    )
    for copy in stores:
        copy.start()
    partial_sums(z, normed, served, group, inner, weight, part)
    sum_parts(cp, part, o_ref, xbuf, qbuf, nbuf, ubuf, rbuf, tbuf)
    for copy in stores:
        copy.wait()
    cp.drain()
    assert cp.used <= SEMS, cp.used


def whole(gate, up, down, gain, prompt, group, inner, weight):
    hbm = pl.BlockSpec(memory_space=pl.ANY)
    out = jax.ShapeDtypeStruct((2048, 256), jnp.bfloat16)
    bf16, f32 = jnp.bfloat16, jnp.float32
    return pl.pallas_call(
        whole_kernel,
        out_shape=(out, out, out, jax.ShapeDtypeStruct((32, 256), bf16)),
        in_specs=[hbm] * 9,
        out_specs=(hbm, hbm, hbm, pl.BlockSpec(memory_space=pltpu.VMEM)),
        scratch_shapes=[
            pltpu.VMEM((3, 32, 32, 32), f32),
            pltpu.VMEM((1, 32), f32),
            pltpu.VMEM((256, 2048), bf16),
            pltpu.VMEM((1, 256), jnp.int32),
            pltpu.VMEM((2, 256), jnp.int32),
            pltpu.VMEM((2, 256), f32),
            pltpu.VMEM((512, 512), bf16),
            pltpu.VMEM((4, 8, 24, 128), bf16),
            pltpu.VMEM((4, 8, 24, 128), bf16),
            pltpu.VMEM((2, 3, 3, 4, 24, 128), bf16),
            pltpu.VMEM((2, 4, 64, 24, 128), bf16),
            pltpu.VMEM((256, 2048), bf16),
            pltpu.VMEM((3, 2048, 256), bf16),
            pltpu.VMEM((2, 4, 8, 32, 256), bf16),
            pltpu.VMEM((4, 8, 32, 256), bf16),
            pltpu.VMEM((4, 8, 32, 256), bf16),
            pltpu.VMEM((3, 8, 32, 256), bf16),
            pltpu.VMEM((32, 256), bf16),
            pltpu.VMEM((2, 4, 32, 256), bf16),
            pltpu.VMEM((2, 3, 32, 256), bf16),
            pltpu.SemaphoreType.DMA((9,)),
            pltpu.SemaphoreType.DMA((3,)),
            pltpu.SemaphoreType.DMA((SEMS,)),
            pltpu.SemaphoreType.DMA((SEMS,)),
        ],
        compiler_params=pltpu.CompilerParams(
            collective_id=0, has_side_effects=True, vmem_limit_bytes=58 << 20
        ),
    )(gate, up, down, gain, prompt, group, inner, weight, jnp.asarray(turning(), bf16))


def shards(
    prompt, norm_gain, gate_master, up_master, down_master, group_choice, inner_choice, route_weight
):
    gate, up, down, mixed = whole(
        gate_master,
        up_master,
        down_master,
        norm_gain[None, :],
        prompt,
        group_choice[None, :],
        inner_choice.T,
        route_weight.T,
    )
    return gate, up, down, mixed.T


def solution(mesh):
    in_specs = (
        P("tp", None),
        P("fs"),
        P(None, "fs", "tp"),
        P(None, "fs", "tp"),
        P(None, "fs", "tp"),
        P("tp"),
        P("tp", None),
        P("tp", None),
    )
    out_specs = (P(None, "fs"), P(None, "fs"), P(None, "fs"), P("tp", "fs"))
    return jax.shard_map(
        shards, mesh=mesh, in_specs=in_specs, out_specs=out_specs, check_vma=False
    )
```

time: 107 us -> 103 us (0.963)
  Pallas kernels: 104 us -> 95.9 us
  local copies, waits for them, and re-layouts: 0.63 us -> 5.54 us
    pallas_call x3 -> x1, Pallas kernels: 104 us -> 95.9 us  [whole(): pl.pallas_call(whole_kernel, out_shape=(out, out, out, jax.ShapeDtypeStru...]
    unnamed x11 -> x10, local copies, waits for them, and re-layouts: 0.63 us -> 5.54 us
where the time goes in v2:
time: 103 us; the launch traced here: 102 us
  Pallas kernels  95.9 us (93%)
  local copies, waits for them, and re-layouts  5.54 us (5%)
    pallas_call x1, Pallas kernels, whole(): pl.pallas_call(whole_kernel, out_shape=(out, out, out, jax.ShapeDtypeStru...  95.9 us
    unnamed x10, local copies, waits for them, and re-layouts  5.54 us

profile of v2, /device:TPU:1, one launch (start us, length us, event | category | flops | bytes accessed | tf_op | source)
XLA Modules:
  0.0 102.1 jit_solution(16011849931702345415)
XLA Ops:
  0.6 95.9 %shard_map.120 = (bf16[2048,256]{1,0:T(8,128)(2,1)}, bf16[2048,256]{1,0:T(8,128)(2,1)}, bf16[2048,256]{1,0:T(8,128)(2,1)}, bf16[32,256]{1,0:T(8,128)(2,1)}) custom-call(f32[32,32,32]{2,1,0:T(8,128)} %gate_hbm.1, f32[32,32,32]{2,1,0:T(8,128)} %up_hbm.1, f32[32,32,32]{2,1,0:T(8,128)} %down_hbm.1, f32[1,32]{1,0:T(1,128)} %bitcast.9, ...), custom_call_target="tpu_custom_call" | custom-call | tf_op jit(solution)/shard_map/pallas_call | solution.py:604
  96.5 0.0 copy-start.1
  96.5 2.4 %copy.17 = bf16[2048,256]{1,0:T(8,128)(2,1)} copy(bf16[2048,256]{1,0:T(8,128)(2,1)} %get-tuple-element.16) | data formatting | bytes 2097152
  98.9 0.0 copy-done.1
  98.9 0.0 copy-start
  98.9 1.0 copy.18
  99.9 0.6 copy-done
  100.5 0.0 copy-start.2
  100.5 1.0 copy.19
  101.5 0.0 copy-done.2
  101.5 0.6 copy.20
Async XLA Ops:
  96.5 2.4 %copy-start.1 = (bf16[2048,256]{1,0:T(8,128)(2,1)S(1)}, bf16[2048,256]{1,0:T(8,128)(2,1)}, u32[]{:S(2)}) copy-start(bf16[2048,256]{1,0:T(8,128)(2,1)} %get-tuple-element.17) | copy-start | bytes 3145732
  98.9 1.6 %copy-start = (bf16[2048,256]{1,0:T(8,128)(2,1)S(1)}, bf16[2048,256]{1,0:T(8,128)(2,1)}, u32[]{:S(2)}) copy-start(bf16[2048,256]{1,0:T(8,128)(2,1)} %get-tuple-element.18) | copy-start | bytes 3145732
  100.5 1.0 copy-start.2

commit v3 on v2

--- a/solution.py
+++ b/solution.py
@@ -332,7 +332,6 @@
             def d2():
                 y2()
                 u2()
-                settle(w)
 
             return d0, d1, d2
         x1, x2, x3 = ring_x((w, 0), views[0], owns)
@@ -362,7 +361,6 @@
         def t4():
             y3()
             u3()
-            settle(w)
 
         return t0, t1, t2, t3, t4
 
@@ -379,6 +377,8 @@
     for kind, n, m in SCHEDULE:
         if kind == "B":
             stride_step(int(n), int(m))
+        elif kind == "S":
+            settle(int(n))
         else:
             ticks[int(n)][int(m)]()
 
@@ -387,8 +387,8 @@
 SCHEDULE = (
     ("w00", "B24", "B23", "B22", "w10", "w01", "B34")
     + ("B33", "w20", "w11", "w02", "B44", "w30", "w21", "w12", "w03")
-    + ("w40", "w31", "w22", "w13", "w04", "w41", "w32", "w23", "w14")
-    + ("w42", "w33", "w24", "w34")
+    + ("w40", "w31", "w22", "w13", "w04", "w41", "w32", "w23", "S0.")
+    + ("w14", "S1.", "w33", "w24", "S2.", "w42", "S4.", "w34", "S3.")
 )
 SEMS = 208
 
@@ -597,6 +597,44 @@
     assert cp.used <= SEMS, cp.used
 
 
+def put_kernel(*refs):
+    sources, targets, held, load, store = refs[:4], refs[4:8], refs[8:12], refs[12], refs[13]
+    moves = []
+    for i, pieces in ((3, 1), (0, PIECES), (1, PIECES), (2, PIECES)):
+        size = sources[i].shape[0] // pieces
+        for n in range(pieces):
+            rows, at = pl.ds(n * size, size), len(moves)
+            moves.append(
+                (
+                    pltpu.make_async_copy(sources[i].at[rows], held[i].at[rows], load.at[at]),
+                    pltpu.make_async_copy(held[i].at[rows], targets[i].at[rows], store.at[at]),
+                )
+            )
+    for get, _ in moves:
+        get.start()
+    for get, give in moves:
+        get.wait()
+        give.start()
+    for _, give in moves:
+        give.wait()
+
+
+PIECES = 4
+
+
+def put(*values):
+    hbm = pl.BlockSpec(memory_space=pl.ANY)
+    return pl.pallas_call(
+        put_kernel,
+        out_shape=tuple(jax.ShapeDtypeStruct(v.shape, v.dtype) for v in values),
+        in_specs=[hbm] * 4,
+        out_specs=(hbm,) * 4,
+        scratch_shapes=[pltpu.VMEM(v.shape, v.dtype) for v in values]
+        + [pltpu.SemaphoreType.DMA((3 * PIECES + 1,))] * 2,
+        compiler_params=pltpu.CompilerParams(vmem_limit_bytes=58 << 20),
+    )(*values)
+
+
 def whole(gate, up, down, gain, prompt, group, inner, weight):
     hbm = pl.BlockSpec(memory_space=pl.ANY)
     out = jax.ShapeDtypeStruct((2048, 256), jnp.bfloat16)
@@ -651,6 +689,7 @@
         inner_choice.T,
         route_weight.T,
     )
+    gate, up, down, mixed = put(gate, up, down, mixed)
     return gate, up, down, mixed.T
 
 

time: 103 us -> 101 us (0.981)
  local copies, waits for them, and re-layouts: 5.54 us -> 0 us
  Pallas kernels: 95.9 us -> 98.7 us
    unnamed x10 -> x0, local copies, waits for them, and re-layouts: 5.54 us -> none
    pallas_call x0 -> x1, Pallas kernels: none -> 2.85 us  [put(): pl.pallas_call(put_kernel, out_shape=tuple((jax.ShapeDtypeStruct(v.shape,...]
where the time goes in v3:
time: 101 us; the launch traced here: 99.3 us
  Pallas kernels  98.7 us (98%)
    pallas_call x1, Pallas kernels, whole(): pl.pallas_call(whole_kernel, out_shape=(out, out, out, jax.ShapeDtypeStru...  95.9 us
    pallas_call x1, Pallas kernels, put(): pl.pallas_call(put_kernel, out_shape=tuple((jax.ShapeDtypeStruct(v.shape,...  2.85 us

profile of v3, /device:TPU:1, one launch (start us, length us, event | category | flops | bytes accessed | tf_op | source)
XLA Modules:
  0.0 99.3 jit_solution(1859188812685577302)
XLA Ops:
  0.6 95.9 %shard_map.120 = (bf16[2048,256]{1,0:T(8,128)(2,1)}, bf16[2048,256]{1,0:T(8,128)(2,1)}, bf16[2048,256]{1,0:T(8,128)(2,1)}, bf16[32,256]{1,0:T(8,128)(2,1)}) custom-call(f32[32,32,32]{2,1,0:T(8,128)} %gate_hbm.1, f32[32,32,32]{2,1,0:T(8,128)} %up_hbm.1, f32[32,32,32]{2,1,0:T(8,128)} %down_hbm.1, f32[1,32]{1,0:T(1,128)} %bitcast.8, ...), custom_call_target="tpu_custom_call" | custom-call | tf_op jit(solution)/shard_map/pallas_call | solution.py:642
  96.5 2.8 %shard_map.121 = (bf16[2048,256]{1,0:T(8,128)(2,1)}, bf16[2048,256]{1,0:T(8,128)(2,1)}, bf16[2048,256]{1,0:T(8,128)(2,1)}, bf16[32,256]{1,0:T(8,128)(2,1)}) custom-call(bf16[2048,256]{1,0:T(8,128)(2,1)} %get-tuple-element.12.refs_0_, bf16[2048,256]{1,0:T(8,128)(2,1)} %get-tuple-element.13.refs_1_, bf16[2048,256]{1,0:T(8,128)(2,1)} %get-tuple-element.14.refs_2_, ...), custom_call_target="tpu_custom_call" | custom-call | tf_op jit(solution)/shard_map/pallas_call | solution.py:627
